TPU v7x, 32 devices: a whole 2x2x4 slice. The times are simulated.
32 devices in a mesh: sp: 4 (over z), dp: 8 (over y, x, core).
Axes of the slice: x: 2, y: 2, z: 4, core: 2. Of those that a mesh axis runs over, the one named last changes fastest.
Arguments:
- inputs: bfloat16 [8, 544, 2048], P('dp', 'sp'), may hold values from -6 to 6
- query_vectors: bfloat16 [8, 544, 1024], P('dp', 'sp'), may hold values from -6 to 6
- key_vectors: bfloat16 [8, 544, 1024], P('dp', 'sp'), may hold values from -6 to 6
- value_vectors: bfloat16 [8, 544, 1024], P('dp', 'sp'), may hold values from -6 to 6
- cotangent: bfloat16 [8, 544, 1024], P('dp', 'sp'), may hold values from -6 to 6
- gate_prefix: float32 [8, 16, 544], P('dp', 'sp'), may hold values from -544 to 0, as said below
- value_weight: bfloat16 [2048, 1024], P('sp', 'dp'), may hold values from -0.125 to 0.125
Outputs:
- query_grad: bfloat16 [8, 544, 1024], P('dp', 'sp')
- key_grad: bfloat16 [8, 544, 1024], P('dp', 'sp')
- input_grad: bfloat16 [8, 544, 2048], P('dp', 'sp')
- weight_grad: float32 [2048, 1024], P('sp', 'dp')
Inputs may be any that keep to these rules, and one draw needn't show every extreme that they name: `gate_prefix`: non-increasing along the positions of each sequence and head.
All inputs are finite; a program needn't handle non-finite values.
Results may differ from a plain program's by a relative error of at most 0.015.
Values may be sent and summed in bfloat16 or wider, within the bound.
A program may use at most 128 MiB of HBM per device.

v0:
```python
import jax
import jax.numpy as jnp
from jax import lax
from jax.sharding import PartitionSpec as P

HEAD_DIM = 64


def attention_backward(query_heads, key_heads, value_heads, grad_heads, prefix):
    length = query_heads.shape[0]
    score_scale = HEAD_DIM ** (-0.5)
    block_count = max(1, length // 512)
    block_rows = length // block_count
    key_accum = jnp.zeros(key_heads.shape, jnp.float32)
    value_accum = jnp.zeros(key_heads.shape, jnp.float32)
    query_parts = []
    for block_index in range(block_count):
        first_row = block_index * block_rows
        last_row = first_row + block_rows
        query_rows = query_heads[first_row:last_row]
        key_rows = key_heads[:last_row]
        grad_rows = grad_heads[first_row:last_row]
        scores = (
            jnp.einsum("qhd,khd->hqk", query_rows, key_rows, preferred_element_type=jnp.float32)
            * score_scale
        )
        scores = scores + prefix[:, first_row:last_row, None] - prefix[:, None, :last_row]
        causal = jnp.arange(last_row)[None, :] <= (first_row + jnp.arange(block_rows))[:, None]
        scores = jnp.where(causal[None], scores, -jnp.inf)
        row_peak = jnp.max(scores, axis=-1, keepdims=True)
        raised_scores = jnp.exp(scores - row_peak)
        softmax_rows = raised_scores / jnp.sum(raised_scores, axis=-1, keepdims=True)
        softmax_low = softmax_rows.astype(jnp.bfloat16)
        value_accum = value_accum.at[:last_row].add(
            jnp.einsum("hqk,qhd->khd", softmax_low, grad_rows, preferred_element_type=jnp.float32)
        )
        softmax_grad = jnp.einsum(
            "qhd,khd->hqk", grad_rows, value_heads[:last_row], preferred_element_type=jnp.float32
        )
        row_term = jnp.sum(softmax_rows * softmax_grad, axis=-1, keepdims=True)
        score_low = (softmax_rows * (softmax_grad - row_term)).astype(jnp.bfloat16)
        query_parts.append(
            (
                jnp.einsum("hqk,khd->qhd", score_low, key_rows, preferred_element_type=jnp.float32)
                * score_scale
            ).astype(jnp.bfloat16)
        )
        key_accum = key_accum.at[:last_row].add(
            jnp.einsum("hqk,qhd->khd", score_low, query_rows, preferred_element_type=jnp.float32)
        )
    query_grad = jnp.concatenate(query_parts, axis=0)
    key_grad = (key_accum * score_scale).astype(jnp.bfloat16)
    return (query_grad, key_grad, value_accum.astype(jnp.bfloat16))


def shards(inputs, query_vectors, key_vectors, value_vectors, cotangent, gate_prefix, value_weight):
    query_seq, key_seq, value_seq, grad_seq, input_cols = (
        lax.all_to_all(query_vectors[0], "sp", split_axis=1, concat_axis=0, tiled=True),
        lax.all_to_all(key_vectors[0], "sp", split_axis=1, concat_axis=0, tiled=True),
        lax.all_to_all(value_vectors[0], "sp", split_axis=1, concat_axis=0, tiled=True),
        lax.all_to_all(cotangent[0], "sp", split_axis=1, concat_axis=0, tiled=True),
        lax.all_to_all(inputs[0], "sp", split_axis=1, concat_axis=0, tiled=True),
    )
    length = query_seq.shape[0]
    local_width = query_seq.shape[1]
    head_shape = (length, local_width // HEAD_DIM, HEAD_DIM)
    query_heads, key_heads, value_heads = attention_backward(
        query_seq.reshape(head_shape),
        key_seq.reshape(head_shape),
        value_seq.reshape(head_shape),
        grad_seq.reshape(head_shape),
        gate_prefix[0],
    )
    query_flat = query_heads.reshape(length, local_width)
    key_flat = key_heads.reshape(length, local_width)
    value_flat = value_heads.reshape(length, local_width)
    value_all = lax.all_gather(value_flat, "sp", axis=1, tiled=True)
    weight_block = lax.all_gather(value_weight, "dp", axis=1, tiled=True)
    weight_rows = lax.psum_scatter(
        lax.dot_general(
            value_all, input_cols, (((0,), (0,)), ((), ())), preferred_element_type=jnp.float32
        ).astype(jnp.bfloat16),
        "dp",
        scatter_dimension=0,
        tiled=True,
    ).astype(jnp.float32)
    weight_grad = weight_rows.T
    query_back, key_back = (
        lax.all_to_all(query_flat, "sp", split_axis=0, concat_axis=1, tiled=True),
        lax.all_to_all(key_flat, "sp", split_axis=0, concat_axis=1, tiled=True),
    )
    column_grad = lax.dot_general(
        value_all, weight_block, (((1,), (1,)), ((), ())), preferred_element_type=jnp.float32
    ).astype(jnp.bfloat16)
    input_grad = lax.all_to_all(column_grad, "sp", split_axis=0, concat_axis=1, tiled=True)
    return (query_back[None], key_back[None], input_grad[None], weight_grad)


def solution(mesh):
    in_specs = (
        P("dp", "sp", None),
        P("dp", "sp", None),
        P("dp", "sp", None),
        P("dp", "sp", None),
        P("dp", "sp", None),
        P("dp", "sp", None),
        P("sp", "dp"),
    )
    out_specs = (P("dp", "sp", None), P("dp", "sp", None), P("dp", "sp", None), P("sp", "dp"))
    return jax.shard_map(shards, mesh=mesh, in_specs=in_specs, out_specs=out_specs, check_vma=False)
```

profile of v0, /device:TPU:0, one launch (start us, length us, event | category | flops | bytes accessed | tf_op | source)
XLA Modules:
  0.0 171.9 jit_solution(9864498030525884451)
XLA Ops:
  7.2 1.2 all_to_all.96
  8.3 0.7 copy.61
  9.1 6.3 %all-to-all-start = ((bf16[136,4,256]{2,0,1:T(8,128)(2,1)}), bf16[136,4,256]{2,0,1:T(8,128)(2,1)S(1)}, u32[]{:S(2)}, u32[]{:S(2)}) async-start(bf16[136,4,256]{2,0,1:T(8,128)(2,1)} %copy.61), calls=%async_computation | async-start | bytes 557056 | tf_op jit(solution)/shard_map/all_to_all | solution.py:58
  15.4 1.2 all_to_all.99
  16.6 0.7 copy.62
  17.3 7.4 %all-to-all-done = bf16[136,4,256]{2,0,1:T(8,128)(2,1)S(1)} async-done(((bf16[136,4,256]{2,0,1:T(8,128)(2,1)}), bf16[136,4,256]{2,0,1:T(8,128)(2,1)S(1)}, u32[]{:S(2)}, u32[]{:S(2)}) %all-to-all-start) | async-done | bytes 278560 | tf_op jit(solution)/shard_map/all_to_all | solution.py:58
  24.7 3.5 %all-to-all-start.1 = ((bf16[136,4,256]{2,0,1:T(8,128)(2,1)}), bf16[136,4,256]{2,0,1:T(8,128)(2,1)S(1)}, u32[]{:S(2)}, u32[]{:S(2)}) async-start(bf16[136,4,256]{2,0,1:T(8,128)(2,1)} %copy.62), calls=%async_computation.1 | async-start | bytes 557056 | tf_op jit(solution)/shard_map/all_to_all | solution.py:59
  28.1 1.2 all_to_all.102
  29.3 0.7 copy.65
  30.1 5.2 %all-to-all-done.1 = bf16[136,4,256]{2,0,1:T(8,128)(2,1)S(1)} async-done(((bf16[136,4,256]{2,0,1:T(8,128)(2,1)}), bf16[136,4,256]{2,0,1:T(8,128)(2,1)S(1)}, u32[]{:S(2)}, u32[]{:S(2)}) %all-to-all-start.1) | async-done | bytes 278560 | tf_op jit(solution)/shard_map/all_to_all | solution.py:59
  35.3 3.5 %all-to-all-start.2 = ((bf16[136,4,256]{2,0,1:T(8,128)(2,1)}), bf16[136,4,256]{2,0,1:T(8,128)(2,1)S(1)}, u32[]{:S(2)}, u32[]{:S(2)}) async-start(bf16[136,4,256]{2,0,1:T(8,128)(2,1)} %copy.65), calls=%async_computation.2 | async-start | bytes 557056 | tf_op jit(solution)/shard_map/all_to_all | solution.py:61
  38.7 0.0 all-gather.3.cloned.1.call-start
  38.8 0.1 iota_compare_fusion
  38.9 0.3 reshape.148
  39.2 0.4 copy.63
  39.5 0.3 reshape.149
  39.8 0.4 copy.64
  40.2 5.4 %all-to-all-done.2 = bf16[136,4,256]{2,0,1:T(8,128)(2,1)S(1)} async-done(((bf16[136,4,256]{2,0,1:T(8,128)(2,1)}), bf16[136,4,256]{2,0,1:T(8,128)(2,1)S(1)}, u32[]{:S(2)}, u32[]{:S(2)}) %all-to-all-start.2) | async-done | bytes 278560 | tf_op jit(solution)/shard_map/all_to_all | solution.py:61
  45.6 0.3 reshape.150
  45.9 0.4 copy.67
  46.2 0.0 copy-done.4
  46.3 4.4 %fusion.22 = (f32[4,544]{1,0:T(4,128)S(1)}, f32[4,544,544]{1,2,0:T(8,128)}) fusion(f32[4,544]{1,0:T(4,128)S(1)} %bitcast.46, pred[544,544]{0,1:T(8,128)(4,1)S(1)} %iota_compare_fusion, bf16[544,4,64]{0,2,1:T(8,128)(2,1)S(1)} %copy.63, bf16[544,4,64]{0,2,1:T(8,128)(2,1)S(1)} %copy.64), kind=kOutput, calls=%fused_computation.30 | convolution fusion | flops 158622240 | bytes 5605376 | tf_op jit(solution)/shard_map/sub | solution.py:31
  50.6 3.8 %fusion.11 = bf16[4,544,64]{1,2,0:T(8,128)(2,1)} fusion(bf16[544,4,64]{0,2,1:T(8,128)(2,1)S(1)} %copy.67, f32[4,544]{1,0:T(4,128)S(1)} %get-tuple-element.60, f32[4,544]{1,0:T(4,128)S(1)} %bitcast.47, pred[544,544]{0,1:T(8,128)(4,1)S(1)} %iota_compare_fusion, bf16[544,4,64]{0,2,1:T(8,128)(2,1)S(1)} %copy.63, bf16[544,4,64]{0,2,1:T(8,128)(2,1)S(1)} %copy.64), kind=kOutput, calls=%fused_computation.21 | convolution fusion | flops 311466656 | bytes 1427456 | tf_op jit(solution)/shard_map/hqk,qhd->khd/dot_general | solution.py:35
  54.5 0.0 all-gather.3.cloned.1.call-update
  54.5 0.2 all_to_all.105
  54.7 0.7 copy.66
  55.4 3.5 %all-to-all-start.3 = ((bf16[136,4,256]{2,0,1:T(8,128)(2,1)}), bf16[136,4,256]{2,0,1:T(8,128)(2,1)S(1)}, u32[]{:S(2)}, u32[]{:S(2)}) async-start(bf16[136,4,256]{2,0,1:T(8,128)(2,1)} %copy.66), calls=%async_computation.3 | async-start | bytes 557056 | tf_op jit(solution)/shard_map/all_to_all | solution.py:60
  58.9 0.0 all-gather.5.cloned.1.call-start
  59.0 0.7 all-gather.5.cloned.1.call-update
  59.7 0.4 all_to_all.116
  60.1 0.9 copy.80
  61.0 5.0 %all-to-all-done.3 = bf16[136,4,256]{2,0,1:T(8,128)(2,1)S(1)} async-done(((bf16[136,4,256]{2,0,1:T(8,128)(2,1)}), bf16[136,4,256]{2,0,1:T(8,128)(2,1)S(1)}, u32[]{:S(2)}, u32[]{:S(2)}) %all-to-all-start.3) | async-done | bytes 278560 | tf_op jit(solution)/shard_map/all_to_all | solution.py:60
  65.9 10.5 %all-to-all-start.7 = ((bf16[136,4,512]{2,0,1:T(8,128)(2,1)}), bf16[136,4,512]{2,0,1:T(8,128)(2,1)}, u32[]{:S(2)}, u32[]{:S(2)}) async-start(bf16[136,4,512]{2,0,1:T(8,128)(2,1)} %copy.80), calls=%async_computation.7 | async-start | bytes 1114112 | tf_op jit(solution)/shard_map/all_to_all | solution.py:62
  76.5 0.3 reshape.151
  76.7 3.5 %multiply_reduce_fusion = (f32[4,544]{1,0:T(4,128)S(1)}, f32[4,544,544]{1,2,0:T(8,128)S(1)}) fusion(f32[4,544,544]{1,2,0:T(8,128)} %get-tuple-element.61, f32[4,544]{1,0:T(4,128)S(1)} %get-tuple-element.60, bf16[544,4,64]{0,2,1:T(8,128)(2,1)S(1)} %copy.67, bf16[544,4,64]{2,1,0:T(4,128)(2,1)S(1)} %reshape.151), kind=kOutput, calls=%fused_computation.2 | convolution fusion | flops 155068288 | bytes 10044416 | tf_op jit(solution)/shard_map/qhd,khd->hqk/dot_general | solution.py:37
  80.2 3.6 %multiply_convert_fusion = bf16[4,544,544]{1,2,0:T(8,128)(2,1)S(1)} fusion(f32[4,544,544]{1,2,0:T(8,128)S(1)} %get-tuple-element.63, f32[4,544]{1,0:T(4,128)S(1)} %get-tuple-element.62, f32[4,544,544]{1,2,0:T(8,128)} %get-tuple-element.61, f32[4,544]{1,0:T(4,128)S(1)} %get-tuple-element.60), kind=kLoop, calls=%fused_computation.1 | loop fusion | flops 4734976 | bytes 11854848 | tf_op jit(solution)/shard_map/convert_element_type | solution.py:41
  83.8 1.7 fusion.15
  85.5 1.3 reshape.153
  86.8 1.0 copy.86
  87.8 12.1 %all-to-all-done.7 = bf16[136,4,512]{2,0,1:T(8,128)(2,1)} async-done(((bf16[136,4,512]{2,0,1:T(8,128)(2,1)}), bf16[136,4,512]{2,0,1:T(8,128)(2,1)}, u32[]{:S(2)}, u32[]{:S(2)}) %all-to-all-start.7) | async-done | bytes 557088 | tf_op jit(solution)/shard_map/all_to_all | solution.py:62
  99.9 4.1 %all-to-all-start.5 = ((bf16[4,136,256]{2,1,0:T(8,128)(2,1)}), bf16[4,136,256]{2,1,0:T(8,128)(2,1)}, u32[]{:S(2)}, u32[]{:S(2)}) async-start(bf16[4,136,256]{2,1,0:T(8,128)(2,1)} %copy.86), calls=%async_computation.5 | async-start | bytes 557056 | tf_op jit(solution)/shard_map/all_to_all | solution.py:90
  104.0 0.2 reduce-scatter.2.cloned.1.call-start
  104.3 0.0 all-gather.3.cloned.1.call-done
  104.3 3.4 %convolution_convert_fusion = bf16[1024,512]{1,0:T(8,128)(2,1)} fusion(bf16[544,1024]{0,1:T(8,128)(2,1)} %all-gather.3.cloned.1.call-done, bf16[544,512]{1,0:T(8,128)(2,1)} %bitcast.14), kind=kOutput, calls=%fused_computation.14 | convolution fusion | flops 570949632 | bytes 2719744 | tf_op jit(solution)/shard_map/dot_general | solution.py:80
  107.7 0.0 reduce-scatter.2.cloned.1.call-update
  107.7 0.7 fusion.14
  108.4 0.4 reshape.152
  108.8 1.0 copy.85
  109.8 1.2 all-to-all-done.5
  111.0 3.6 %all-to-all-start.4 = ((bf16[4,136,256]{2,1,0:T(8,128)(2,1)}), bf16[4,136,256]{2,1,0:T(8,128)(2,1)S(1)}, u32[]{:S(2)}, u32[]{:S(2)}) async-start(bf16[4,136,256]{2,1,0:T(8,128)(2,1)} %copy.85), calls=%async_computation.4 | async-start | bytes 557056 | tf_op jit(solution)/shard_map/all_to_all | solution.py:89
  114.6 9.8 %all-gather.5.cloned.1.call-done = bf16[512,1024]{1,0:T(8,128)(2,1)} async-done(((bf16[512,128]{1,0:T(8,128)(2,1)}), bf16[512,1024]{1,0:T(8,128)(2,1)}) %all-gather.5.cloned.1.call-update) | async-done | bytes 1048592 | tf_op jit(solution)/shard_map/all_gather | solution.py:78
  124.4 3.4 %convolution_convert_fusion.1 = bf16[544,512]{1,0:T(8,128)(2,1)} fusion(bf16[544,1024]{0,1:T(8,128)(2,1)} %all-gather.3.cloned.1.call-done, bf16[512,1024]{1,0:T(8,128)(2,1)} %all-gather.5.cloned.1.call-done), kind=kOutput, calls=%fused_computation.16 | convolution fusion | flops 570703872 | bytes 2719744 | tf_op jit(solution)/shard_map/dot_general | solution.py:92
  127.8 0.0 all-to-all-done.4
  127.8 4.6 %all-to-all-start.6 = ((bf16[4,136,512]{2,1,0:T(8,128)(2,1)}), bf16[4,136,512]{2,1,0:T(8,128)(2,1)S(1)}, u32[]{:S(2)}, u32[]{:S(2)}) async-start(bf16[4,136,512]{2,1,0:T(8,128)(2,1)} %bitcast.11), calls=%async_computation.6 | async-start | bytes 1114112 | tf_op jit(solution)/shard_map/all_to_all | solution.py:95
  132.4 1.1 copy.76
  133.5 0.9 broadcast_in_dim.30
  134.3 0.1 copy.72
  134.5 0.9 broadcast_in_dim.29
  135.4 12.6 %all-to-all-done.6 = bf16[4,136,512]{2,1,0:T(8,128)(2,1)S(1)} async-done(((bf16[4,136,512]{2,1,0:T(8,128)(2,1)}), bf16[4,136,512]{2,1,0:T(8,128)(2,1)S(1)}, u32[]{:S(2)}, u32[]{:S(2)}) %all-to-all-start.6) | async-done | bytes 557088 | tf_op jit(solution)/shard_map/all_to_all | solution.py:95
  148.0 0.3 copy.79
  148.3 1.2 broadcast_in_dim.31
  149.5 14.1 %reduce-scatter.2.cloned.1.call-done = bf16[128,512]{1,0:T(8,128)(2,1)} async-done(((bf16[1024,512]{1,0:T(8,128)(2,1)}), bf16[128,512]{1,0:T(8,128)(2,1)}) %reduce-scatter.2.cloned.1.call-update) | async-done | bytes 131088 | tf_op jit(solution)/shard_map/reduce_scatter | solution.py:79
  163.6 0.9 convert_bitcast_fusion
  164.5 0.8 copy.81
  (9 shorter events, 0.0 us)
Async XLA Ops:
  7.2 39.1 %copy-start.4 = (f32[1,4,544]{2,1,0:T(4,128)S(1)}, f32[1,4,544]{2,1,0:T(4,128)}, u32[]{:S(2)}) copy-start(f32[1,4,544]{2,1,0:T(4,128)} %param.20) | copy-start | bytes 26116
  9.1 15.6 %all-to-all-start = ((bf16[136,4,256]{2,0,1:T(8,128)(2,1)}), bf16[136,4,256]{2,0,1:T(8,128)(2,1)S(1)}, u32[]{:S(2)}, u32[]{:S(2)}) async-start(bf16[136,4,256]{2,0,1:T(8,128)(2,1)} %copy.61), calls=%async_computation | async-start | bytes 557056 | tf_op jit(solution)/shard_map/all_to_all | solution.py:58
  24.7 10.6 %all-to-all-start.1 = ((bf16[136,4,256]{2,0,1:T(8,128)(2,1)}), bf16[136,4,256]{2,0,1:T(8,128)(2,1)S(1)}, u32[]{:S(2)}, u32[]{:S(2)}) async-start(bf16[136,4,256]{2,0,1:T(8,128)(2,1)} %copy.62), calls=%async_computation.1 | async-start | bytes 557056 | tf_op jit(solution)/shard_map/all_to_all | solution.py:59
  35.3 10.3 %all-to-all-start.2 = ((bf16[136,4,256]{2,0,1:T(8,128)(2,1)}), bf16[136,4,256]{2,0,1:T(8,128)(2,1)S(1)}, u32[]{:S(2)}, u32[]{:S(2)}) async-start(bf16[136,4,256]{2,0,1:T(8,128)(2,1)} %copy.65), calls=%async_computation.2 | async-start | bytes 557056 | tf_op jit(solution)/shard_map/all_to_all | solution.py:61
  38.7 65.5 %all-gather.3.cloned.1.call-start = ((), (), s32[]{:S(2)}) async-start(), calls=%async_computation.9 | async-start | bytes 1638400 | tf_op jit(solution)/shard_map/all_gather | solution.py:77
  40.2 10.5 %copy-start = (bf16[544,4,64]{0,2,1:T(8,128)(2,1)}, bf16[544,4,64]{0,2,1:T(8,128)(2,1)S(1)}, u32[]{:S(2)}) copy-start(bf16[544,4,64]{0,2,1:T(8,128)(2,1)S(1)} %copy.64) | copy-start | bytes 835588
  50.6 3.9 %copy-start.3 = (bf16[1,136,1024]{2,1,0:T(8,128)(2,1)S(1)}, bf16[1,136,1024]{2,1,0:T(8,128)(2,1)}, u32[]{:S(2)}) copy-start(bf16[1,136,1024]{2,1,0:T(8,128)(2,1)} %param.18) | copy-start | bytes 835588
  50.6 9.0 %copy-start.2 = (bf16[1,136,2048]{2,1,0:T(8,128)(2,1)S(1)}, bf16[1,136,2048]{2,1,0:T(8,128)(2,1)}, u32[]{:S(2)}) copy-start(bf16[1,136,2048]{2,1,0:T(8,128)(2,1)} %param.15) | copy-start | bytes 1671172
  55.4 10.5 %all-to-all-start.3 = ((bf16[136,4,256]{2,0,1:T(8,128)(2,1)}), bf16[136,4,256]{2,0,1:T(8,128)(2,1)S(1)}, u32[]{:S(2)}, u32[]{:S(2)}) async-start(bf16[136,4,256]{2,0,1:T(8,128)(2,1)} %copy.66), calls=%async_computation.3 | async-start | bytes 557056 | tf_op jit(solution)/shard_map/all_to_all | solution.py:60
  58.9 65.5 %all-gather.5.cloned.1.call-start = ((), (), s32[]{:S(2)}) async-start(), calls=%async_computation.10 | async-start | bytes 1179648 | tf_op jit(solution)/shard_map/all_gather | solution.py:78
  65.9 34.0 %all-to-all-start.7 = ((bf16[136,4,512]{2,0,1:T(8,128)(2,1)}), bf16[136,4,512]{2,0,1:T(8,128)(2,1)}, u32[]{:S(2)}, u32[]{:S(2)}) async-start(bf16[136,4,512]{2,0,1:T(8,128)(2,1)} %copy.80), calls=%async_computation.7 | async-start | bytes 1114112 | tf_op jit(solution)/shard_map/all_to_all | solution.py:62
  87.8 19.9 %copy-start.1 = (bf16[544,4,64]{0,2,1:T(8,128)(2,1)S(1)}, bf16[544,4,64]{0,2,1:T(8,128)(2,1)}, u32[]{:S(2)}) copy-start(bf16[544,4,64]{0,2,1:T(8,128)(2,1)} %copy-done) | copy-start | bytes 835588
  99.9 11.1 %all-to-all-start.5 = ((bf16[4,136,256]{2,1,0:T(8,128)(2,1)}), bf16[4,136,256]{2,1,0:T(8,128)(2,1)}, u32[]{:S(2)}, u32[]{:S(2)}) async-start(bf16[4,136,256]{2,1,0:T(8,128)(2,1)} %copy.86), calls=%async_computation.5 | async-start | bytes 557056 | tf_op jit(solution)/shard_map/all_to_all | solution.py:90
  104.0 59.6 %reduce-scatter.2.cloned.1.call-start = ((), (), s32[]{:S(2)}) async-start(), calls=%async_computation.11 | async-start | bytes 1179648 | tf_op jit(solution)/shard_map/reduce_scatter | solution.py:79
  111.0 16.8 %all-to-all-start.4 = ((bf16[4,136,256]{2,1,0:T(8,128)(2,1)}), bf16[4,136,256]{2,1,0:T(8,128)(2,1)S(1)}, u32[]{:S(2)}, u32[]{:S(2)}) async-start(bf16[4,136,256]{2,1,0:T(8,128)(2,1)} %copy.85), calls=%async_computation.4 | async-start | bytes 557056 | tf_op jit(solution)/shard_map/all_to_all | solution.py:89
  127.8 20.2 %all-to-all-start.6 = ((bf16[4,136,512]{2,1,0:T(8,128)(2,1)}), bf16[4,136,512]{2,1,0:T(8,128)(2,1)S(1)}, u32[]{:S(2)}, u32[]{:S(2)}) async-start(bf16[4,136,512]{2,1,0:T(8,128)(2,1)} %bitcast.11), calls=%async_computation.6 | async-start | bytes 1114112 | tf_op jit(solution)/shard_map/all_to_all | solution.py:95
Sparse Core Ops, SparseCore 0:
  54.6 45.5 all-gather.2
  102.0 22.3 all-gather.4
  127.6 35.9 reduce-scatter.1
where the time goes:
time: 173 us; the launch traced here: 172 us
  waiting for transfers between devices  73.5 us (42%)
  starting transfers between devices  39.8 us (23%)
  matrix products  20.9 us (12%)
  local copies, waits for them, and re-layouts  19.1 us (11%)
  between operations  14 us (8%)
  other arithmetic  4.58 us (3%)
    reduce_scatter x1, waiting for transfers between devices, shards(): lax.psum_scatter(lax.dot_general(value_all, input_cols, (((0,), (0,)), ((...  14.1 us
    all_to_all x1, waiting for transfers between devices, shards(): lax.all_to_all(column_grad, 'sp', split_axis=0, concat_axis=1, tiled=True)  12.6 us
    all_to_all x1, waiting for transfers between devices, shards(): lax.all_to_all(inputs[0], 'sp', split_axis=1, concat_axis=0, tiled=True)  12.1 us
    all_to_all x1, starting transfers between devices, shards(): lax.all_to_all(inputs[0], 'sp', split_axis=1, concat_axis=0, tiled=True)  10.5 us
    all_gather x1, waiting for transfers between devices, shards(): weight_block = lax.all_gather(value_weight, 'dp', axis=1, tiled=True)  9.81 us
    all_to_all x1, waiting for transfers between devices, shards(): lax.all_to_all(query_vectors[0], 'sp', split_axis=1, concat_axis=0, tiled...  7.36 us
    all_to_all x1, starting transfers between devices, shards(): lax.all_to_all(query_vectors[0], 'sp', split_axis=1, concat_axis=0, tiled...  6.35 us
    all_to_all x1, waiting for transfers between devices, shards(): lax.all_to_all(cotangent[0], 'sp', split_axis=1, concat_axis=0, tiled=True)  5.43 us
  transfers between devices with their start and end apart: 11, of which 9 were waited for; matrix products, arithmetic and copies ran while one was open for 17% of the time, Pallas kernels for 0%

commit v1 on v0

--- a/solution.py
+++ b/solution.py
@@ -1,6 +1,10 @@
+import functools
+
 import jax
 import jax.numpy as jnp
 from jax import lax
+from jax.experimental import pallas as pl
+from jax.experimental.pallas import tpu as pltpu
 from jax.sharding import PartitionSpec as P
 
 HEAD_DIM = 64
@@ -96,6 +100,286 @@
     return (query_back[None], key_back[None], input_grad[None], weight_grad)
 
 
+LANES = 128
+MESH = pl.DeviceIdType.MESH
+
+
+def one_kernel_fits(sp_count, dp_count, inputs, query, key, value, cotangent, gate, weight):
+    rows, width = query.shape[1:]
+    model = inputs.shape[2]
+    return (
+        dp_count == 8
+        and width == dp_count * LANES
+        and width % (sp_count * LANES) == 0
+        and LANES == 2 * HEAD_DIM
+        and rows % 8 == 0
+        and model % (sp_count * LANES) == 0
+        and model % (2 * LANES) == 0
+        and sp_count % 2 == 0
+        and rows * sp_count <= 1024
+        and (dp_count * rows + width) * model <= 3 * 2**21
+    )
+
+
+def attention_pair(q32, k32, v32, g32, rows_of, columns_of, stats):
+    length = q32.shape[0]
+    scale = HEAD_DIM ** (-0.5)
+    dot = functools.partial(lax.dot_general, preferred_element_type=jnp.float32)
+    dq_ref, dk_ref, dv_ref = stats
+    lane = lax.broadcasted_iota(jnp.int32, (length, LANES), 1)
+    q_all = q32.astype(jnp.bfloat16)
+    g_all = g32.astype(jnp.bfloat16)
+    for head in range(2):
+        own = (lane < HEAD_DIM) if head == 0 else (lane >= HEAD_DIM)
+        q_own, k_own, v_own, g_own = (
+            jnp.where(own, x, 0.0).astype(jnp.bfloat16) for x in (q32, k32, v32, g32)
+        )
+        gate_row, gate_column = rows_of[head], columns_of[head]
+        first = 0
+        while first < length:
+            last = min(first + 256, length)
+            size = last - first
+            scores = dot(k_own[:last], q_all[first:last], (((1,), (1,)), ((), ()))) * scale
+            scores = scores + gate_row[:, first:last] - gate_column[:last]
+            key_pos = lax.broadcasted_iota(jnp.int32, (last, size), 0)
+            query_pos = lax.broadcasted_iota(jnp.int32, (last, size), 1) + first
+            scores = jnp.where(key_pos <= query_pos, scores, -jnp.inf)
+            peak = jnp.max(scores, axis=0, keepdims=True)
+            raised = jnp.exp(scores - peak)
+            soft = raised * (1.0 / jnp.sum(raised, axis=0, keepdims=True))
+            soft_grad = dot(v_own[:last], g_all[first:last], (((1,), (1,)), ((), ())))
+            row_term = jnp.sum(soft * soft_grad, axis=0, keepdims=True)
+            score_low = (soft * (soft_grad - row_term)).astype(jnp.bfloat16)
+            dv = dot(soft.astype(jnp.bfloat16), g_own[first:last], (((1,), (0,)), ((), ())))
+            dk = dot(score_low, q_own[first:last], (((1,), (0,)), ((), ()))) * scale
+            dq = dot(score_low, k_own[:last], (((0,), (0,)), ((), ()))) * scale
+            seen = first if head == 0 else last
+            if seen:
+                dv_ref[:seen] += dv[:seen]
+                dk_ref[:seen] += dk[:seen]
+            if seen < last:
+                dv_ref[seen:last] = dv[seen:]
+                dk_ref[seen:last] = dk[seen:]
+            if head == 0:
+                dq_ref[first:last] = dq
+            else:
+                dq_ref[first:last] += dq
+            first = last
+
+
+def kernel(
+    n, groups, in_ref, q_ref, k_ref, v_ref, g_ref, gate_ref, w_ref,
+    qg_ref, kg_ref, ig_ref, wg_ref,
+    pair_in, pair_out, vg, vg_seq, x_all, w_all, part, part_in, gate_pad, gate_t,
+    dq_ref, dk_ref, dv_ref, send_sems, recv_sems,
+):
+    s = lax.axis_index("sp")
+    d = lax.axis_index("dp")
+    core, x, y = d % 2, (d // 2) % 2, d // 4
+    rows = q_ref.shape[0]
+    length = n * rows
+    half = in_ref.shape[1] // 2
+
+    def near(step):
+        return (
+            d
+            + (step % 2) * (1 - 2 * core)
+            + ((step // 2) % 2) * (2 - 4 * x)
+            + (step // 4) * (4 - 8 * y)
+        )
+
+    partner, x_near, y_near, corner = near(1), near(2), near(4), near(6)
+    started = []
+
+    def send(src, dst, to_sp, to_dp):
+        index = len(started)
+        copy = pltpu.make_async_remote_copy(
+            src_ref=src,
+            dst_ref=dst,
+            send_sem=send_sems.at[index],
+            recv_sem=recv_sems.at[index],
+            device_id={"sp": to_sp, "dp": to_dp},
+            device_id_type=MESH,
+        )
+        copy.start()
+        started.append(copy)
+        return copy
+
+    barrier = pltpu.get_barrier_semaphore()
+    for r in range(1, n):
+        pl.semaphore_signal(barrier, inc=1, device_id={"sp": (s + r) % n, "dp": d}, device_id_type=MESH)
+    for step in range(1, 8):
+        pl.semaphore_signal(barrier, inc=1, device_id={"sp": s, "dp": near(step)}, device_id_type=MESH)
+    pl.semaphore_wait(barrier, n - 1 + 7)
+
+    arrived = []
+    for p in range(groups):
+        for a, ref in enumerate((q_ref, k_ref, v_ref, g_ref)):
+            for r in range(1, n):
+                to = (s + r) % n
+                columns = pl.ds(pl.multiple_of((to * groups + p) * LANES, LANES), LANES)
+                arrived.append(send(ref.at[:, columns], pair_in.at[p, a, s], to, d))
+    x_near0 = send(in_ref, x_all.at[d], s, x_near)
+    y_near0 = send(in_ref, x_all.at[d], s, y_near)
+    x_part0 = send(in_ref, x_all.at[d], s, partner)
+    w_came = [send(w_ref, w_all.at[d, s], (s + r) % n, d) for r in range(1, n)]
+
+    for p in range(groups):
+        columns = pl.ds(pl.multiple_of((s * groups + p) * LANES, LANES), LANES)
+        for a, ref in enumerate((q_ref, k_ref, v_ref, g_ref)):
+            pair_in[p, a, s] = ref[:, columns]
+    x_all[d] = in_ref[...]
+    w_all[d, s] = w_ref[...]
+    gate_pad[...] = jnp.zeros_like(gate_pad)
+    gate_pad[: gate_ref.shape[0], :length] = gate_ref[...]
+    gate_t[...] = gate_pad[...].T
+
+    back_v, back_qk = [], []
+
+    def attend(p):
+        for copy in arrived[p * 4 * (n - 1) : (p + 1) * 4 * (n - 1)]:
+            copy.wait_recv()
+        wide = [pair_in[p, a].astype(jnp.float32).reshape(length, LANES) for a in range(4)]
+        heads = (2 * p, 2 * p + 1)
+        attention_pair(
+            *wide,
+            [gate_pad[h : h + 1, :length] for h in heads],
+            [gate_t[:length, h : h + 1] for h in heads],
+            (dq_ref, dk_ref, dv_ref),
+        )
+        for a, ref in enumerate((dv_ref, dq_ref, dk_ref)):
+            pair_out[p, a] = ref[...].reshape(n, rows, LANES).astype(jnp.bfloat16)
+        columns = pl.ds(pl.multiple_of((s * groups + p) * LANES, LANES), LANES)
+        for a, ref in enumerate((None, qg_ref, kg_ref)):
+            for r in range(1, n):
+                to = (s + r) % n
+                if a == 0:
+                    back_v.append(send(pair_out.at[p, a, to], vg.at[s * groups + p], to, d))
+                else:
+                    back_qk.append(send(pair_out.at[p, a, to], ref.at[:, columns], to, d))
+            if a == 0:
+                vg[s * groups + p] = pair_out[p, a, s]
+            else:
+                ref[:, columns] = pair_out[p, a, s]
+
+    def spread_middle(buffer, low, high, from_x, from_y):
+        from_x.wait_recv()
+        a = send(low(x_near), low(x_near), s, y_near)
+        b = send(buffer.at[x_near], buffer.at[x_near], s, partner)
+        from_y.wait_recv()
+        c = send(high(y_near), high(y_near), s, x_near)
+        e = send(buffer.at[y_near], buffer.at[y_near], s, partner)
+        return a, c, b, e
+
+    def spread_last(buffer, middle):
+        middle[0].wait_recv()
+        middle[1].wait_recv()
+        return send(buffer.at[corner], buffer.at[corner], s, partner)
+
+    x_low = lambda i: x_all.at[i, :, pl.ds(0, half)]
+    x_high = lambda i: x_all.at[i, :, pl.ds(half, half)]
+    w_low = lambda i: w_all.at[i, pl.ds(0, n // 2)]
+    w_high = lambda i: w_all.at[i, pl.ds(n // 2, n // 2)]
+
+    x_middle = x_last = None
+    for p in range(groups):
+        attend(p)
+        if p == 0:
+            x_middle = spread_middle(x_all, x_low, x_high, x_near0, y_near0)
+    x_last = spread_last(x_all, x_middle)
+
+    for copy in w_came:
+        copy.wait_recv()
+    w_x = send(w_all.at[d], w_all.at[d], s, x_near)
+    w_y = send(w_all.at[d], w_all.at[d], s, y_near)
+    w_part = send(w_all.at[d], w_all.at[d], s, partner)
+
+    for copy in back_v:
+        copy.wait_recv()
+    moved = [send(vg.at[near(step)], vg_seq.at[d], s, near(step)) for step in range(1, 8)]
+    vg_seq[d] = vg[d]
+    for copy in moved:
+        copy.wait_recv()
+    for copy in (x_part0, x_middle[2], x_middle[3], x_last):
+        copy.wait_recv()
+
+    block = in_ref.shape[1] // n
+    dot = functools.partial(lax.dot_general, preferred_element_type=jnp.float32)
+    for j in range(n):
+        total = None
+        for i in range(8):
+            term = dot(vg_seq[i], x_all[i, :, j * block : (j + 1) * block], (((0,), (0,)), ((), ())))
+            total = term if total is None else total + term
+        part[j] = total.astype(jnp.bfloat16)
+    sums = [send(part.at[(s + r) % n], part_in.at[r - 1], (s + r) % n, d) for r in range(1, n)]
+
+    w_middle = spread_middle(w_all, w_low, w_high, w_x, w_y)
+    w_last = spread_last(w_all, w_middle)
+    for copy in (w_part, w_middle[2], w_middle[3], w_last):
+        copy.wait_recv()
+    vg_rows = jnp.concatenate([vg[i] for i in range(8)], axis=1)
+    for j in range(n):
+        w_rows = jnp.concatenate([w_all[i, j] for i in range(8)], axis=1)
+        ig_ref[:, j * block : (j + 1) * block] = dot(
+            vg_rows, w_rows, (((1,), (1,)), ((), ()))
+        ).astype(jnp.bfloat16)
+
+    total = part[s].astype(jnp.float32)
+    for r, copy in enumerate(sums):
+        copy.wait_recv()
+        total = total + part_in[r].astype(jnp.float32)
+    wg_ref[...] = total.T
+    for copy in back_qk:
+        copy.wait_recv()
+    for copy in started:
+        copy.wait_send()
+
+
+def fused(mesh, inputs, query, key, value, cotangent, gate, weight):
+    n = mesh.shape["sp"]
+    rows, width = query.shape[1:]
+    model = inputs.shape[2]
+    groups = width // (n * LANES)
+    length = n * rows
+    padded = -(-length // LANES) * LANES
+    bf16, f32 = jnp.bfloat16, jnp.float32
+    copies = (n - 1) * (4 * groups + 1 + 3 * groups + 1) + 2 * 8 + 7
+    vmem = pl.BlockSpec(memory_space=pltpu.VMEM)
+    outs = pl.pallas_call(
+        functools.partial(kernel, n, groups),
+        out_shape=(
+            jax.ShapeDtypeStruct((rows, width), bf16),
+            jax.ShapeDtypeStruct((rows, width), bf16),
+            jax.ShapeDtypeStruct((rows, model), bf16),
+            jax.ShapeDtypeStruct((model // n, LANES), f32),
+        ),
+        in_specs=[vmem] * 7,
+        out_specs=(vmem,) * 4,
+        scratch_shapes=[
+            pltpu.VMEM((groups, 4, n, rows, LANES), bf16),
+            pltpu.VMEM((groups, 3, n, rows, LANES), bf16),
+            pltpu.VMEM((8, rows, LANES), bf16),
+            pltpu.VMEM((8, rows, LANES), bf16),
+            pltpu.VMEM((8, rows, model), bf16),
+            pltpu.VMEM((8, n, model // n, LANES), bf16),
+            pltpu.VMEM((n, LANES, model // n), bf16),
+            pltpu.VMEM((n - 1, LANES, model // n), bf16),
+            pltpu.VMEM((LANES, padded), f32),
+            pltpu.VMEM((padded, LANES), f32),
+            pltpu.VMEM((length, LANES), f32),
+            pltpu.VMEM((length, LANES), f32),
+            pltpu.VMEM((length, LANES), f32),
+            pltpu.SemaphoreType.DMA((copies,)),
+            pltpu.SemaphoreType.DMA((copies,)),
+        ],
+        compiler_params=pltpu.CompilerParams(
+            collective_id=0, has_side_effects=True, vmem_limit_bytes=60 * 2**20
+        ),
+    )(inputs[0], query[0], key[0], value[0], cotangent[0], gate[0], weight)
+    query_grad, key_grad, input_grad, weight_grad = outs
+    return (query_grad[None], key_grad[None], input_grad[None], weight_grad)
+
+
 def solution(mesh):
     in_specs = (
         P("dp", "sp", None),
@@ -107,4 +391,11 @@
         P("sp", "dp"),
     )
     out_specs = (P("dp", "sp", None), P("dp", "sp", None), P("dp", "sp", None), P("sp", "dp"))
-    return jax.shard_map(shards, mesh=mesh, in_specs=in_specs, out_specs=out_specs, check_vma=False)
+    sp_count, dp_count = mesh.shape["sp"], mesh.shape["dp"]
+
+    def per_device(*arrays):
+        if one_kernel_fits(sp_count, dp_count, *arrays):
+            return fused(mesh, *arrays)
+        return shards(*arrays)
+
+    return jax.shard_map(per_device, mesh=mesh, in_specs=in_specs, out_specs=out_specs, check_vma=False)

time: 173 us -> 85.3 us (0.49)
  the two profiles are of different devices: /device:TPU:0 before, /device:TPU:29 now
where the time goes in v1:
time: 85.3 us; the launch traced here: 85.1 us
  Pallas kernels  80.1 us (94%)
  local copies, waits for them, and re-layouts  4.27 us (5%)
    pallas_call x1, Pallas kernels, fused(): pl.pallas_call(functools.partial(kernel, n, groups), out_shape=(jax.Shape...  80.1 us
    unnamed x10, local copies, waits for them, and re-layouts  4.27 us

profile of v1, /device:TPU:29, one launch (start us, length us, event | category | flops | bytes accessed | tf_op | source)
XLA Modules:
  0.0 85.1 jit_solution(8391482091791583190)
XLA Ops:
  0.6 80.1 %shard_map.102 = (bf16[136,1024]{1,0:T(8,128)(2,1)}, bf16[136,1024]{1,0:T(8,128)(2,1)}, bf16[136,2048]{1,0:T(8,128)(2,1)}, f32[512,128]{1,0:T(8,128)}) custom-call(bf16[136,2048]{1,0:T(8,128)(2,1)} %bitcast.9, bf16[136,1024]{1,0:T(8,128)(2,1)} %bitcast.11, bf16[136,1024]{1,0:T(8,128)(2,1)} %bitcast.12, bf16[136,1024]{1,0:T(8,128)(2,1)} %bitcast.13, ...), custom_call_target="tpu_custom_call" | custom-call | tf_op jit(solution)/shard_map/pallas_call | solution.py:348
  80.8 0.0 copy-start.1
  80.8 0.0 copy-start
  80.8 1.8 %copy.15 = bf16[1,136,1024]{2,1,0:T(8,128)(2,1)} copy(bf16[1,136,1024]{2,1,0:T(8,128)(2,1)} %bitcast.16) | data formatting | bytes 557056
  82.6 0.0 copy-done.1
  82.6 0.7 copy.16
  83.3 0.0 copy-done
  83.3 0.0 copy-start.2
  83.3 0.8 copy.17
  84.1 0.3 copy-done.2
  84.4 0.7 copy.18
Async XLA Ops:
  80.8 1.8 %copy-start.1 = (bf16[136,1024]{1,0:T(8,128)(2,1)S(1)}, bf16[136,1024]{1,0:T(8,128)(2,1)}, u32[]{:S(2)}) copy-start(bf16[136,1024]{1,0:T(8,128)(2,1)} %get-tuple-element.9) | copy-start | bytes 835588
  80.8 2.5 %copy-start = (bf16[136,2048]{1,0:T(8,128)(2,1)S(1)}, bf16[136,2048]{1,0:T(8,128)(2,1)}, u32[]{:S(2)}) copy-start(bf16[136,2048]{1,0:T(8,128)(2,1)} %get-tuple-element.10) | copy-start | bytes 1671172
  83.3 1.1 %copy-start.2 = (f32[512,128]{1,0:T(8,128)S(1)}, f32[512,128]{1,0:T(8,128)}, u32[]{:S(2)}) copy-start(f32[512,128]{1,0:T(8,128)} %get-tuple-element.19) | copy-start | bytes 786436

commit v2 on v1

--- a/solution.py
+++ b/solution.py
@@ -121,57 +121,80 @@
     )
 
 
-def attention_pair(q32, k32, v32, g32, rows_of, columns_of, stats):
+def query_blocks(length):
+    return [(first, min(first + 256, length)) for first in range(0, length, 256)]
+
+
+def own_lanes(head, *arrays):
+    lane = lax.broadcasted_iota(jnp.int32, arrays[0].shape, 1)
+    own = (lane < HEAD_DIM) if head == 0 else (lane >= HEAD_DIM)
+    return [jnp.where(own, x, 0.0).astype(jnp.bfloat16) for x in arrays]
+
+
+def add_block(ref, value, seen):
+    if seen:
+        ref[:seen] += value[:seen]
+    if seen < value.shape[0]:
+        ref[seen : value.shape[0]] = value[seen:]
+
+
+dot = functools.partial(lax.dot_general, preferred_element_type=jnp.float32)
+BY_LANES = (((1,), (1,)), ((), ()))
+BY_ROWS = (((0,), (0,)), ((), ()))
+PLAIN = (((1,), (0,)), ((), ()))
+
+
+def softmax_pair(q32, k32, g32, gate_rows, gate_columns, soft_refs, dv_ref):
     length = q32.shape[0]
     scale = HEAD_DIM ** (-0.5)
-    dot = functools.partial(lax.dot_general, preferred_element_type=jnp.float32)
-    dq_ref, dk_ref, dv_ref = stats
-    lane = lax.broadcasted_iota(jnp.int32, (length, LANES), 1)
     q_all = q32.astype(jnp.bfloat16)
-    g_all = g32.astype(jnp.bfloat16)
     for head in range(2):
-        own = (lane < HEAD_DIM) if head == 0 else (lane >= HEAD_DIM)
-        q_own, k_own, v_own, g_own = (
-            jnp.where(own, x, 0.0).astype(jnp.bfloat16) for x in (q32, k32, v32, g32)
-        )
-        gate_row, gate_column = rows_of[head], columns_of[head]
-        first = 0
-        while first < length:
-            last = min(first + 256, length)
+        k_own, g_own = own_lanes(head, k32, g32)
+        for first, last in query_blocks(length):
             size = last - first
-            scores = dot(k_own[:last], q_all[first:last], (((1,), (1,)), ((), ()))) * scale
-            scores = scores + gate_row[:, first:last] - gate_column[:last]
+            scores = dot(k_own[:last], q_all[first:last], BY_LANES) * scale
+            scores = scores + gate_rows[head][:, first:last] - gate_columns[head][:last]
             key_pos = lax.broadcasted_iota(jnp.int32, (last, size), 0)
             query_pos = lax.broadcasted_iota(jnp.int32, (last, size), 1) + first
             scores = jnp.where(key_pos <= query_pos, scores, -jnp.inf)
             peak = jnp.max(scores, axis=0, keepdims=True)
             raised = jnp.exp(scores - peak)
             soft = raised * (1.0 / jnp.sum(raised, axis=0, keepdims=True))
-            soft_grad = dot(v_own[:last], g_all[first:last], (((1,), (1,)), ((), ())))
+            soft_refs[head][:last, first:last] = soft
+            add_block(
+                dv_ref, dot(soft.astype(jnp.bfloat16), g_own[first:last], PLAIN),
+                first if head == 0 else last,
+            )
+
+
+def gradient_pair(q32, k32, v32, g32, soft_refs, dq_ref, dk_ref):
+    length = q32.shape[0]
+    scale = HEAD_DIM ** (-0.5)
+    g_all = g32.astype(jnp.bfloat16)
+    for head in range(2):
+        q_own, k_own, v_own = own_lanes(head, q32, k32, v32)
+        for first, last in query_blocks(length):
+            soft = soft_refs[head][:last, first:last]
+            soft_grad = dot(v_own[:last], g_all[first:last], BY_LANES)
             row_term = jnp.sum(soft * soft_grad, axis=0, keepdims=True)
             score_low = (soft * (soft_grad - row_term)).astype(jnp.bfloat16)
-            dv = dot(soft.astype(jnp.bfloat16), g_own[first:last], (((1,), (0,)), ((), ())))
-            dk = dot(score_low, q_own[first:last], (((1,), (0,)), ((), ()))) * scale
-            dq = dot(score_low, k_own[:last], (((0,), (0,)), ((), ()))) * scale
-            seen = first if head == 0 else last
-            if seen:
-                dv_ref[:seen] += dv[:seen]
-                dk_ref[:seen] += dk[:seen]
-            if seen < last:
-                dv_ref[seen:last] = dv[seen:]
-                dk_ref[seen:last] = dk[seen:]
+            add_block(
+                dk_ref, dot(score_low, q_own[first:last], PLAIN) * scale,
+                first if head == 0 else last,
+            )
+            dq = dot(score_low, k_own[:last], BY_ROWS) * scale
             if head == 0:
                 dq_ref[first:last] = dq
             else:
                 dq_ref[first:last] += dq
-            first = last
 
 
 def kernel(
-    n, groups, in_ref, q_ref, k_ref, v_ref, g_ref, gate_ref, w_ref,
+    n, groups, in_hbm, q_hbm, k_hbm, v_hbm, g_hbm, gate_ref, w_hbm,
     qg_ref, kg_ref, ig_ref, wg_ref,
+    in_ref, q_ref, k_ref, v_ref, g_ref, w_ref,
     pair_in, pair_out, vg, vg_seq, x_all, w_all, part, part_in, gate_pad, gate_t,
-    dq_ref, dk_ref, dv_ref, send_sems, recv_sems,
+    soft, dq_ref, dk_ref, dv_ref, local_sems, hop_sems, hop_recv_sems, send_sems, recv_sems,
 ):
     s = lax.axis_index("sp")
     d = lax.axis_index("dp")
@@ -179,6 +202,15 @@
     rows = q_ref.shape[0]
     length = n * rows
     half = in_ref.shape[1] // 2
+
+    fetched = [
+        pltpu.make_async_copy(src, dst, local_sems.at[i])
+        for i, (src, dst) in enumerate(
+            ((w_hbm, w_ref), (q_hbm, q_ref), (k_hbm, k_ref), (g_hbm, g_ref), (in_hbm, in_ref), (v_hbm, v_ref))
+        )
+    ]
+    for copy in fetched:
+        copy.start()
 
     def near(step):
         return (
@@ -205,62 +237,107 @@
         started.append(copy)
         return copy
 
+    def lanes_of(device, p):
+        return pl.ds(pl.multiple_of((device * groups + p) * LANES, LANES), LANES)
+
     barrier = pltpu.get_barrier_semaphore()
     for r in range(1, n):
         pl.semaphore_signal(barrier, inc=1, device_id={"sp": (s + r) % n, "dp": d}, device_id_type=MESH)
     for step in range(1, 8):
         pl.semaphore_signal(barrier, inc=1, device_id={"sp": s, "dp": near(step)}, device_id_type=MESH)
     pl.semaphore_wait(barrier, n - 1 + 7)
-
-    arrived = []
-    for p in range(groups):
-        for a, ref in enumerate((q_ref, k_ref, v_ref, g_ref)):
-            for r in range(1, n):
-                to = (s + r) % n
-                columns = pl.ds(pl.multiple_of((to * groups + p) * LANES, LANES), LANES)
-                arrived.append(send(ref.at[:, columns], pair_in.at[p, a, s], to, d))
+    for copy in fetched:
+        copy.wait()
+
+    def hop(t, up):
+        block = (s - t + 1 + n) % n if up else (s + t - 1) % n
+        src = w_ref if t == 1 else w_all.at[d, block]
+        index = 2 * (t - 1) + int(up)
+        return pltpu.make_async_remote_copy(
+            src_ref=src,
+            dst_ref=w_all.at[d, block],
+            send_sem=hop_sems.at[index],
+            recv_sem=hop_recv_sems.at[index],
+            device_id={"sp": (s + 1) % n if up else (s - 1 + n) % n, "dp": d},
+            device_id_type=MESH,
+        )
+
+    def hop_sends(t, act):
+        pl.when((s >= t - 1) & (s < n - 1))(lambda: act(hop(t, True)))
+        pl.when((s <= n - t) & (s > 0))(lambda: act(hop(t, False)))
+
+    def hop_start(t):
+        hop_sends(t, lambda copy: copy.start())
+
+    def hop_arrive(t):
+        pl.when(s >= t)(lambda: hop(t, True).wait_recv())
+        pl.when(s < n - t)(lambda: hop(t, False).wait_recv())
+
+    def send_pair(p, a, ref):
+        return [
+            send(ref.at[:, lanes_of((s + r) % n, p)], pair_in.at[p, a, s], (s + r) % n, d)
+            for r in range(1, n)
+        ]
+
+    hop_start(1)
+    early = [
+        [c for a, ref in ((0, q_ref), (1, k_ref), (3, g_ref)) for c in send_pair(p, a, ref)]
+        for p in range(groups)
+    ]
     x_near0 = send(in_ref, x_all.at[d], s, x_near)
     y_near0 = send(in_ref, x_all.at[d], s, y_near)
     x_part0 = send(in_ref, x_all.at[d], s, partner)
-    w_came = [send(w_ref, w_all.at[d, s], (s + r) % n, d) for r in range(1, n)]
 
     for p in range(groups):
-        columns = pl.ds(pl.multiple_of((s * groups + p) * LANES, LANES), LANES)
         for a, ref in enumerate((q_ref, k_ref, v_ref, g_ref)):
-            pair_in[p, a, s] = ref[:, columns]
+            pair_in[p, a, s] = ref[:, lanes_of(s, p)]
     x_all[d] = in_ref[...]
     w_all[d, s] = w_ref[...]
     gate_pad[...] = jnp.zeros_like(gate_pad)
     gate_pad[: gate_ref.shape[0], :length] = gate_ref[...]
     gate_t[...] = gate_pad[...].T
 
-    back_v, back_qk = [], []
-
-    def attend(p):
-        for copy in arrived[p * 4 * (n - 1) : (p + 1) * 4 * (n - 1)]:
+    def wide(p, a):
+        return pair_in[p, a].astype(jnp.float32).reshape(length, LANES)
+
+    def give_back(p, a, ref):
+        pair_out[p, a] = ref[...].reshape(n, rows, LANES).astype(jnp.bfloat16)
+        copies = []
+        for r in range(1, n):
+            to = (s + r) % n
+            dst = (
+                vg.at[s * groups + p] if a == 0
+                else (None, qg_ref, kg_ref)[a].at[:, lanes_of(s, p)]
+            )
+            copies.append(send(pair_out.at[p, a, to], dst, to, d))
+        return copies
+
+    def first_half(p):
+        for copy in early[p]:
             copy.wait_recv()
-        wide = [pair_in[p, a].astype(jnp.float32).reshape(length, LANES) for a in range(4)]
+
+    def softmax_part(p):
         heads = (2 * p, 2 * p + 1)
-        attention_pair(
-            *wide,
+        softmax_pair(
+            wide(p, 0), wide(p, 1), wide(p, 3),
             [gate_pad[h : h + 1, :length] for h in heads],
             [gate_t[:length, h : h + 1] for h in heads],
-            (dq_ref, dk_ref, dv_ref),
-        )
-        for a, ref in enumerate((dv_ref, dq_ref, dk_ref)):
-            pair_out[p, a] = ref[...].reshape(n, rows, LANES).astype(jnp.bfloat16)
-        columns = pl.ds(pl.multiple_of((s * groups + p) * LANES, LANES), LANES)
-        for a, ref in enumerate((None, qg_ref, kg_ref)):
-            for r in range(1, n):
-                to = (s + r) % n
-                if a == 0:
-                    back_v.append(send(pair_out.at[p, a, to], vg.at[s * groups + p], to, d))
-                else:
-                    back_qk.append(send(pair_out.at[p, a, to], ref.at[:, columns], to, d))
-            if a == 0:
-                vg[s * groups + p] = pair_out[p, a, s]
-            else:
-                ref[:, columns] = pair_out[p, a, s]
+            [soft.at[h] for h in heads],
+            dv_ref,
+        )
+        copies = give_back(p, 0, dv_ref)
+        vg[s * groups + p] = pair_out[p, 0, s]
+        return copies
+
+    def gradient_part(p):
+        gradient_pair(
+            wide(p, 0), wide(p, 1), wide(p, 2), wide(p, 3),
+            [soft.at[2 * p], soft.at[2 * p + 1]], dq_ref, dk_ref,
+        )
+        copies = give_back(p, 1, dq_ref) + give_back(p, 2, dk_ref)
+        qg_ref[:, lanes_of(s, p)] = pair_out[p, 1, s]
+        kg_ref[:, lanes_of(s, p)] = pair_out[p, 2, s]
+        return copies
 
     def spread_middle(buffer, low, high, from_x, from_y):
         from_x.wait_recv()
@@ -281,48 +358,68 @@
     w_low = lambda i: w_all.at[i, pl.ds(0, n // 2)]
     w_high = lambda i: w_all.at[i, pl.ds(n // 2, n // 2)]
 
-    x_middle = x_last = None
+    back_v, back_qk, late = [], [], []
+    x_middle = None
+    hop_next = 1
+
+    def relay():
+        nonlocal hop_next
+        if hop_next < n:
+            hop_arrive(hop_next)
+            if hop_next + 1 < n:
+                hop_start(hop_next + 1)
+            hop_next += 1
+
+    relay()
     for p in range(groups):
-        attend(p)
+        first_half(p)
+        if p == 0:
+            late = [send_pair(i, 2, v_ref) for i in range(groups)]
+        back_v += softmax_part(p)
+        relay()
         if p == 0:
             x_middle = spread_middle(x_all, x_low, x_high, x_near0, y_near0)
-    x_last = spread_last(x_all, x_middle)
-
-    for copy in w_came:
-        copy.wait_recv()
+    while hop_next < n:
+        relay()
     w_x = send(w_all.at[d], w_all.at[d], s, x_near)
     w_y = send(w_all.at[d], w_all.at[d], s, y_near)
     w_part = send(w_all.at[d], w_all.at[d], s, partner)
+    x_last = spread_last(x_all, x_middle)
+
+    for copy in late[0]:
+        copy.wait_recv()
+    back_qk += gradient_part(0)
 
     for copy in back_v:
         copy.wait_recv()
     moved = [send(vg.at[near(step)], vg_seq.at[d], s, near(step)) for step in range(1, 8)]
     vg_seq[d] = vg[d]
+    for p in range(1, groups):
+        for copy in late[p]:
+            copy.wait_recv()
+        back_qk += gradient_part(p)
+    w_middle = spread_middle(w_all, w_low, w_high, w_x, w_y)
+    for copy in (x_part0, x_middle[2], x_middle[3], x_last):
+        copy.wait_recv()
     for copy in moved:
         copy.wait_recv()
-    for copy in (x_part0, x_middle[2], x_middle[3], x_last):
-        copy.wait_recv()
 
     block = in_ref.shape[1] // n
-    dot = functools.partial(lax.dot_general, preferred_element_type=jnp.float32)
     for j in range(n):
         total = None
         for i in range(8):
-            term = dot(vg_seq[i], x_all[i, :, j * block : (j + 1) * block], (((0,), (0,)), ((), ())))
+            term = dot(vg_seq[i], x_all[i, :, j * block : (j + 1) * block], BY_ROWS)
             total = term if total is None else total + term
         part[j] = total.astype(jnp.bfloat16)
     sums = [send(part.at[(s + r) % n], part_in.at[r - 1], (s + r) % n, d) for r in range(1, n)]
 
-    w_middle = spread_middle(w_all, w_low, w_high, w_x, w_y)
     w_last = spread_last(w_all, w_middle)
     for copy in (w_part, w_middle[2], w_middle[3], w_last):
         copy.wait_recv()
     vg_rows = jnp.concatenate([vg[i] for i in range(8)], axis=1)
     for j in range(n):
         w_rows = jnp.concatenate([w_all[i, j] for i in range(8)], axis=1)
-        ig_ref[:, j * block : (j + 1) * block] = dot(
-            vg_rows, w_rows, (((1,), (1,)), ((), ()))
-        ).astype(jnp.bfloat16)
+        ig_ref[:, j * block : (j + 1) * block] = dot(vg_rows, w_rows, BY_LANES).astype(jnp.bfloat16)
 
     total = part[s].astype(jnp.float32)
     for r, copy in enumerate(sums):
@@ -333,6 +430,8 @@
         copy.wait_recv()
     for copy in started:
         copy.wait_send()
+    for t in range(1, n):
+        hop_sends(t, lambda copy: copy.wait_send())
 
 
 def fused(mesh, inputs, query, key, value, cotangent, gate, weight):
@@ -343,8 +442,9 @@
     length = n * rows
     padded = -(-length // LANES) * LANES
     bf16, f32 = jnp.bfloat16, jnp.float32
-    copies = (n - 1) * (4 * groups + 1 + 3 * groups + 1) + 2 * 8 + 7
+    copies = (n - 1) * (7 * groups + 1) + 2 * 8 + 7
     vmem = pl.BlockSpec(memory_space=pltpu.VMEM)
+    hbm = pl.BlockSpec(memory_space=pl.ANY)
     outs = pl.pallas_call(
         functools.partial(kernel, n, groups),
         out_shape=(
@@ -353,9 +453,12 @@
             jax.ShapeDtypeStruct((rows, model), bf16),
             jax.ShapeDtypeStruct((model // n, LANES), f32),
         ),
-        in_specs=[vmem] * 7,
+        in_specs=[hbm] * 5 + [vmem, hbm],
         out_specs=(vmem,) * 4,
         scratch_shapes=[
+            pltpu.VMEM((rows, model), bf16),
+            *[pltpu.VMEM((rows, width), bf16)] * 4,
+            pltpu.VMEM((model // n, LANES), bf16),
             pltpu.VMEM((groups, 4, n, rows, LANES), bf16),
             pltpu.VMEM((groups, 3, n, rows, LANES), bf16),
             pltpu.VMEM((8, rows, LANES), bf16),
@@ -366,9 +469,10 @@
             pltpu.VMEM((n - 1, LANES, model // n), bf16),
             pltpu.VMEM((LANES, padded), f32),
             pltpu.VMEM((padded, LANES), f32),
-            pltpu.VMEM((length, LANES), f32),
-            pltpu.VMEM((length, LANES), f32),
-            pltpu.VMEM((length, LANES), f32),
+            pltpu.VMEM((2 * groups, length, length), f32),
+            *[pltpu.VMEM((length, LANES), f32)] * 3,
+            pltpu.SemaphoreType.DMA((6,)),
+            *[pltpu.SemaphoreType.DMA((2 * (n - 1),))] * 2,
             pltpu.SemaphoreType.DMA((copies,)),
             pltpu.SemaphoreType.DMA((copies,)),
         ],

time: 85.3 us -> 79.2 us (0.928)
  the two profiles are of different devices: /device:TPU:29 before, /device:TPU:0 now
where the time goes in v2:
time: 79.2 us; the launch traced here: 78.1 us
  Pallas kernels  73.2 us (92%)
  local copies, waits for them, and re-layouts  4.27 us (5%)
    pallas_call x1, Pallas kernels, fused(): pl.pallas_call(functools.partial(kernel, n, groups), out_shape=(jax.Shape...  73.2 us
    unnamed x10, local copies, waits for them, and re-layouts  4.27 us

profile of v2, /device:TPU:0, one launch (start us, length us, event | category | flops | bytes accessed | tf_op | source)
XLA Modules:
  0.0 78.1 jit_solution(7885395005127081752)
XLA Ops:
  0.6 73.2 %shard_map.102 = (bf16[136,1024]{1,0:T(8,128)(2,1)}, bf16[136,1024]{1,0:T(8,128)(2,1)}, bf16[136,2048]{1,0:T(8,128)(2,1)}, f32[512,128]{1,0:T(8,128)}) custom-call(bf16[136,2048]{1,0:T(8,128)(2,1)} %bitcast.9, bf16[136,1024]{1,0:T(8,128)(2,1)} %bitcast.11, bf16[136,1024]{1,0:T(8,128)(2,1)} %bitcast.12, bf16[136,1024]{1,0:T(8,128)(2,1)} %bitcast.13, ...), custom_call_target="tpu_custom_call" | custom-call | tf_op jit(solution)/shard_map/pallas_call | solution.py:448
  73.8 0.0 copy-start.1
  73.9 0.0 copy-start
  73.9 1.8 %copy.15 = bf16[1,136,1024]{2,1,0:T(8,128)(2,1)} copy(bf16[1,136,1024]{2,1,0:T(8,128)(2,1)} %bitcast.16) | data formatting | bytes 557056
  75.6 0.0 copy-done.1
  75.6 0.7 copy.16
  76.3 0.0 copy-done
  76.3 0.0 copy-start.2
  76.3 0.8 %copy.17 = bf16[1,136,2048]{2,1,0:T(8,128)(2,1)} copy(bf16[1,136,2048]{2,1,0:T(8,128)(2,1)S(1)} %bitcast.10) | data formatting | bytes 1114112
  77.1 0.3 copy-done.2
  77.4 0.7 copy.18
Async XLA Ops:
  73.8 1.8 %copy-start.1 = (bf16[136,1024]{1,0:T(8,128)(2,1)S(1)}, bf16[136,1024]{1,0:T(8,128)(2,1)}, u32[]{:S(2)}) copy-start(bf16[136,1024]{1,0:T(8,128)(2,1)} %get-tuple-element.9) | copy-start | bytes 835588
  73.9 2.5 %copy-start = (bf16[136,2048]{1,0:T(8,128)(2,1)S(1)}, bf16[136,2048]{1,0:T(8,128)(2,1)}, u32[]{:S(2)}) copy-start(bf16[136,2048]{1,0:T(8,128)(2,1)} %get-tuple-element.10) | copy-start | bytes 1671172
  76.3 1.1 %copy-start.2 = (f32[512,128]{1,0:T(8,128)S(1)}, f32[512,128]{1,0:T(8,128)}, u32[]{:S(2)}) copy-start(f32[512,128]{1,0:T(8,128)} %get-tuple-element.19) | copy-start | bytes 786436

commit v3 on v2

--- a/solution.py
+++ b/solution.py
@@ -280,10 +280,15 @@
         ]
 
     hop_start(1)
-    early = [
-        [c for a, ref in ((0, q_ref), (1, k_ref), (3, g_ref)) for c in send_pair(p, a, ref)]
-        for p in range(groups)
-    ]
+    early = [[] for _ in range(groups)]
+    queue = [(p, a, ref) for p in range(groups) for a, ref in ((0, q_ref), (1, k_ref), (3, g_ref))]
+
+    def send_early(count):
+        for p, a, ref in queue[:count]:
+            early[p].extend(send_pair(p, a, ref))
+        del queue[:count]
+
+    send_early(2)
     x_near0 = send(in_ref, x_all.at[d], s, x_near)
     y_near0 = send(in_ref, x_all.at[d], s, y_near)
     x_part0 = send(in_ref, x_all.at[d], s, partner)
@@ -371,34 +376,35 @@
             hop_next += 1
 
     relay()
+    send_early(2)
+    relay()
+    send_early(len(queue))
+    x_middle = spread_middle(x_all, x_low, x_high, x_near0, y_near0)
     for p in range(groups):
+        if p == groups - 1:
+            while hop_next < n:
+                relay()
+            w_x = send(w_all.at[d], w_all.at[d], s, x_near)
+            w_y = send(w_all.at[d], w_all.at[d], s, y_near)
+            w_part = send(w_all.at[d], w_all.at[d], s, partner)
+            x_last = spread_last(x_all, x_middle)
         first_half(p)
-        if p == 0:
-            late = [send_pair(i, 2, v_ref) for i in range(groups)]
         back_v += softmax_part(p)
-        relay()
-        if p == 0:
-            x_middle = spread_middle(x_all, x_low, x_high, x_near0, y_near0)
-    while hop_next < n:
-        relay()
-    w_x = send(w_all.at[d], w_all.at[d], s, x_near)
-    w_y = send(w_all.at[d], w_all.at[d], s, y_near)
-    w_part = send(w_all.at[d], w_all.at[d], s, partner)
-    x_last = spread_last(x_all, x_middle)
-
-    for copy in late[0]:
-        copy.wait_recv()
-    back_qk += gradient_part(0)
-
-    for copy in back_v:
-        copy.wait_recv()
-    moved = [send(vg.at[near(step)], vg_seq.at[d], s, near(step)) for step in range(1, 8)]
-    vg_seq[d] = vg[d]
-    for p in range(1, groups):
+        late.append(send_pair(p, 2, v_ref))
+
+    for p in range(groups - 1):
         for copy in late[p]:
             copy.wait_recv()
         back_qk += gradient_part(p)
+
+    for copy in back_v:
+        copy.wait_recv()
+    moved = [send(vg.at[near(step)], vg_seq.at[d], s, near(step)) for step in range(1, 8)]
+    vg_seq[d] = vg[d]
     w_middle = spread_middle(w_all, w_low, w_high, w_x, w_y)
+    for copy in late[groups - 1]:
+        copy.wait_recv()
+    back_qk += gradient_part(groups - 1)
     for copy in (x_part0, x_middle[2], x_middle[3], x_last):
         copy.wait_recv()
     for copy in moved:
@@ -445,14 +451,15 @@
     copies = (n - 1) * (7 * groups + 1) + 2 * 8 + 7
     vmem = pl.BlockSpec(memory_space=pltpu.VMEM)
     hbm = pl.BlockSpec(memory_space=pl.ANY)
+    results = (
+        jax.ShapeDtypeStruct((rows, width), bf16),
+        jax.ShapeDtypeStruct((rows, width), bf16),
+        jax.ShapeDtypeStruct((rows, model), bf16),
+        jax.ShapeDtypeStruct((model // n, LANES), f32),
+    )
     outs = pl.pallas_call(
         functools.partial(kernel, n, groups),
-        out_shape=(
-            jax.ShapeDtypeStruct((rows, width), bf16),
-            jax.ShapeDtypeStruct((rows, width), bf16),
-            jax.ShapeDtypeStruct((rows, model), bf16),
-            jax.ShapeDtypeStruct((model // n, LANES), f32),
-        ),
+        out_shape=tuple(pltpu.VMEM(x.shape, x.dtype) for x in results),
         in_specs=[hbm] * 5 + [vmem, hbm],
         out_specs=(vmem,) * 4,
         scratch_shapes=[

time: 79.2 us -> 70 us (0.88); the launches traced: 78.1 us -> 69.8 us
  Pallas kernels: 73.2 us -> 66.3 us
  local copies, waits for them, and re-layouts: 4.27 us -> 2.92 us
    pallas_call x1, Pallas kernels: 73.2 us -> 66.3 us  [fused(): pl.pallas_call(functools.partial(kernel, n, groups), out_shape=tuple((plt...]
    unnamed x10 -> x4, local copies, waits for them, and re-layouts: 4.27 us -> 2.92 us
where the time goes in v3:
time: 70 us; the launch traced here: 69.8 us
  Pallas kernels  66.3 us (95%)
  local copies, waits for them, and re-layouts  2.92 us (4%)
    pallas_call x1, Pallas kernels, fused(): pl.pallas_call(functools.partial(kernel, n, groups), out_shape=tuple((plt...  66.3 us
    unnamed x4, local copies, waits for them, and re-layouts  2.92 us

profile of v3, /device:TPU:0, one launch (start us, length us, event | category | flops | bytes accessed | tf_op | source)
XLA Modules:
  0.0 69.8 jit_solution(7594266106265435053)
XLA Ops:
  0.6 66.3 %shard_map.102 = (bf16[136,1024]{1,0:T(8,128)(2,1)S(1)}, bf16[136,1024]{1,0:T(8,128)(2,1)S(1)}, bf16[136,2048]{1,0:T(8,128)(2,1)S(1)}, f32[512,128]{1,0:T(8,128)S(1)}) custom-call(bf16[136,2048]{1,0:T(8,128)(2,1)} %bitcast.12, bf16[136,1024]{1,0:T(8,128)(2,1)} %bitcast.13, bf16[136,1024]{1,0:T(8,128)(2,1)} %bitcast.14, bf16[136,1024]{1,0:T(8,128)(2,1)} %bitcast.15, ...), custom_call_target="tpu_custom_call" | custom-call | tf_op jit(solution)/shard_map/pallas_call | solution.py:460
  66.9 0.7 %copy.15 = bf16[1,136,1024]{2,1,0:T(8,128)(2,1)} copy(bf16[1,136,1024]{2,1,0:T(8,128)(2,1)S(1)} %bitcast.11) | data formatting | bytes 557056
  67.6 0.7 %copy.16 = bf16[1,136,1024]{2,1,0:T(8,128)(2,1)} copy(bf16[1,136,1024]{2,1,0:T(8,128)(2,1)S(1)} %bitcast.10) | data formatting | bytes 557056
  68.3 0.7 %copy.18 = f32[512,128]{1,0:T(8,128)} copy(f32[512,128]{1,0:T(8,128)S(1)} %get-tuple-element.15) | data formatting | bytes 524288
  69.0 0.8 %copy.17 = bf16[1,136,2048]{2,1,0:T(8,128)(2,1)} copy(bf16[1,136,2048]{2,1,0:T(8,128)(2,1)S(1)} %bitcast.9) | data formatting | bytes 1114112

commit v4 on v3

--- a/solution.py
+++ b/solution.py
@@ -411,15 +411,41 @@
         copy.wait_recv()
 
     block = in_ref.shape[1] // n
-    for j in range(n):
+    def weight_part(j):
+        columns = pl.ds(pl.multiple_of(j * block, LANES), block)
         total = None
         for i in range(8):
-            term = dot(vg_seq[i], x_all[i, :, j * block : (j + 1) * block], BY_ROWS)
+            term = dot(vg_seq[i], x_all[i, :, columns], BY_ROWS)
             total = term if total is None else total + term
-        part[j] = total.astype(jnp.bfloat16)
-    sums = [send(part.at[(s + r) % n], part_in.at[r - 1], (s + r) % n, d) for r in range(1, n)]
-
-    w_last = spread_last(w_all, w_middle)
+        return total
+
+    def send_part(j, slot, to):
+        return send(part.at[j], part_in.at[slot], to, d)
+
+    two_steps = n == 4
+    if two_steps:
+        mate, across = s + 1 - 2 * (s % 2), (s + 2) % n
+        far = (mate + 2) % n
+        part[far] = weight_part(far).astype(jnp.bfloat16)
+        far_sum = send_part(far, 0, mate)
+        part[mate] = weight_part(mate).astype(jnp.bfloat16)
+        sums = [send_part(mate, 1, mate)]
+        across_sum = weight_part(across)
+        own_sum = weight_part(s)
+        w_last = spread_last(w_all, w_middle)
+        far_sum.wait_recv()
+        part[across] = (across_sum + part_in[0].astype(jnp.float32)).astype(jnp.bfloat16)
+        sums.append(send_part(across, 2, across))
+    else:
+        sums = []
+        for r in range(1, n):
+            to = (s + r) % n
+            part[to] = weight_part(to).astype(jnp.bfloat16)
+            sums.append(send_part(to, r - 1, to))
+        own_sum = weight_part(s)
+        w_last = spread_last(w_all, w_middle)
+    first_slot = int(two_steps)
+
     for copy in (w_part, w_middle[2], w_middle[3], w_last):
         copy.wait_recv()
     vg_rows = jnp.concatenate([vg[i] for i in range(8)], axis=1)
@@ -427,17 +453,20 @@
         w_rows = jnp.concatenate([w_all[i, j] for i in range(8)], axis=1)
         ig_ref[:, j * block : (j + 1) * block] = dot(vg_rows, w_rows, BY_LANES).astype(jnp.bfloat16)
 
-    total = part[s].astype(jnp.float32)
-    for r, copy in enumerate(sums):
-        copy.wait_recv()
-        total = total + part_in[r].astype(jnp.float32)
-    wg_ref[...] = total.T
     for copy in back_qk:
         copy.wait_recv()
     for copy in started:
-        copy.wait_send()
+        if all(copy is not other for other in sums):
+            copy.wait_send()
     for t in range(1, n):
         hop_sends(t, lambda copy: copy.wait_send())
+    total = own_sum
+    for r, copy in enumerate(sums):
+        copy.wait_recv()
+        total = total + part_in[first_slot + r].astype(jnp.float32)
+    wg_ref[...] = total.T
+    for copy in sums:
+        copy.wait_send()
 
 
 def fused(mesh, inputs, query, key, value, cotangent, gate, weight):

time: 70 us -> 67 us (0.957)
  Pallas kernels: 66.3 us -> 62.9 us
    pallas_call x1, Pallas kernels: 66.3 us -> 62.9 us  [fused(): pl.pallas_call(functools.partial(kernel, n, groups), out_shape=tuple((plt...]
where the time goes in v4:
time: 67 us; the launch traced here: 66.5 us
  Pallas kernels  62.9 us (94%)
  local copies, waits for them, and re-layouts  2.92 us (4%)
    pallas_call x1, Pallas kernels, fused(): pl.pallas_call(functools.partial(kernel, n, groups), out_shape=tuple((plt...  62.9 us
    unnamed x4, local copies, waits for them, and re-layouts  2.92 us

profile of v4, /device:TPU:0, one launch (start us, length us, event | category | flops | bytes accessed | tf_op | source)
XLA Modules:
  0.0 66.5 jit_solution(14510207752426406001)
XLA Ops:
  0.6 62.9 %shard_map.102 = (bf16[136,1024]{1,0:T(8,128)(2,1)S(1)}, bf16[136,1024]{1,0:T(8,128)(2,1)S(1)}, bf16[136,2048]{1,0:T(8,128)(2,1)S(1)}, f32[512,128]{1,0:T(8,128)S(1)}) custom-call(bf16[136,2048]{1,0:T(8,128)(2,1)} %bitcast.12, bf16[136,1024]{1,0:T(8,128)(2,1)} %bitcast.13, bf16[136,1024]{1,0:T(8,128)(2,1)} %bitcast.14, bf16[136,1024]{1,0:T(8,128)(2,1)} %bitcast.15, ...), custom_call_target="tpu_custom_call" | custom-call | tf_op jit(solution)/shard_map/pallas_call | solution.py:489
  63.6 0.7 %copy.15 = bf16[1,136,1024]{2,1,0:T(8,128)(2,1)} copy(bf16[1,136,1024]{2,1,0:T(8,128)(2,1)S(1)} %bitcast.11) | data formatting | bytes 557056
  64.3 0.7 %copy.16 = bf16[1,136,1024]{2,1,0:T(8,128)(2,1)} copy(bf16[1,136,1024]{2,1,0:T(8,128)(2,1)S(1)} %bitcast.10) | data formatting | bytes 557056
  65.0 0.7 %copy.18 = f32[512,128]{1,0:T(8,128)} copy(f32[512,128]{1,0:T(8,128)S(1)} %get-tuple-element.15) | data formatting | bytes 524288
  65.7 0.8 %copy.17 = bf16[1,136,2048]{2,1,0:T(8,128)(2,1)} copy(bf16[1,136,2048]{2,1,0:T(8,128)(2,1)S(1)} %bitcast.9) | data formatting | bytes 1114112

commit v5 on v4

--- a/solution.py
+++ b/solution.py
@@ -467,6 +467,15 @@
     wg_ref[...] = total.T
     for copy in sums:
         copy.wait_send()
+
+
+def put_out(*refs):
+    sems = refs[-1]
+    copies = [pltpu.make_async_copy(refs[i], refs[4 + i], sems.at[i]) for i in range(4)]
+    for copy in copies:
+        copy.start()
+    for copy in copies:
+        copy.wait()
 
 
 def fused(mesh, inputs, query, key, value, cotangent, gate, weight):
@@ -516,7 +525,14 @@
             collective_id=0, has_side_effects=True, vmem_limit_bytes=60 * 2**20
         ),
     )(inputs[0], query[0], key[0], value[0], cotangent[0], gate[0], weight)
-    query_grad, key_grad, input_grad, weight_grad = outs
+    query_grad, key_grad, input_grad, weight_grad = pl.pallas_call(
+        put_out,
+        out_shape=results,
+        in_specs=[vmem] * 4,
+        out_specs=(hbm,) * 4,
+        scratch_shapes=[pltpu.SemaphoreType.DMA((4,))],
+        compiler_params=pltpu.CompilerParams(vmem_limit_bytes=2**20),
+    )(*(pltpu.with_memory_space_constraint(x, pltpu.VMEM) for x in outs))
     return (query_grad[None], key_grad[None], input_grad[None], weight_grad)
 
 

time: 67 us -> 65.1 us (0.972)
  local copies, waits for them, and re-layouts: 2.92 us -> 0 us
  Pallas kernels: 62.9 us -> 64.1 us
    unnamed x4 -> x0, local copies, waits for them, and re-layouts: 2.92 us -> none
    pallas_call x0 -> x1, Pallas kernels: none -> 1.11 us  [fused(): pl.pallas_call(put_out, out_shape=results, in_specs=[vmem] * 4, out_specs...]
where the time goes in v5:
time: 65.1 us; the launch traced here: 64.7 us
  Pallas kernels  64.1 us (98%)
    pallas_call x1, Pallas kernels, fused(): pl.pallas_call(functools.partial(kernel, n, groups), out_shape=tuple((plt...  62.9 us

profile of v5, /device:TPU:0, one launch (start us, length us, event | category | flops | bytes accessed | tf_op | source)
XLA Modules:
  0.0 64.7 jit_solution(12219397840626551692)
XLA Ops:
  0.6 62.9 %shard_map.102 = (bf16[136,1024]{1,0:T(8,128)(2,1)S(1)}, bf16[136,1024]{1,0:T(8,128)(2,1)S(1)}, bf16[136,2048]{1,0:T(8,128)(2,1)S(1)}, f32[512,128]{1,0:T(8,128)S(1)}) custom-call(bf16[136,2048]{1,0:T(8,128)(2,1)} %bitcast.9, bf16[136,1024]{1,0:T(8,128)(2,1)} %bitcast.10, bf16[136,1024]{1,0:T(8,128)(2,1)} %bitcast.11, bf16[136,1024]{1,0:T(8,128)(2,1)} %bitcast.12, ...), custom_call_target="tpu_custom_call" | custom-call | tf_op jit(solution)/shard_map/pallas_call | solution.py:498
  63.6 1.1 %shard_map.103 = (bf16[136,1024]{1,0:T(8,128)(2,1)}, bf16[136,1024]{1,0:T(8,128)(2,1)}, bf16[136,2048]{1,0:T(8,128)(2,1)}, f32[512,128]{1,0:T(8,128)}) custom-call(bf16[136,1024]{1,0:T(8,128)(2,1)S(1)} %get-tuple-element.12.refs_0_, bf16[136,1024]{1,0:T(8,128)(2,1)S(1)} %get-tuple-element.13.refs_1_, bf16[136,2048]{1,0:T(8,128)(2,1)S(1)} %get-tuple-element.14.refs_2_, ...), custom_call_target="tpu_custom_call" | custom-call | tf_op jit(solution)/shard_map/pallas_call | solution.py:528
